TPU v7x, 512 devices: a whole 4x4x16 slice. The times are simulated.
512 devices in a mesh: ep: 32 (over z, core), tp: 16 (over y, x).
Axes of the slice: x: 4, y: 4, z: 16, core: 2. Of those that a mesh axis runs over, the one named last changes fastest.
Arguments:
- tokens: bfloat16 [1024, 2048], P('ep', 'tp'), may hold values from -200 to 200
- routing: int32 [1024, 4], P('ep'), may hold values from 0 to 63, all different within a row; in each aligned block of 32 rows (0 to 31, 32 to 63, ...) at most 8 rows name the same one
- gate_weights: float32 [1024, 4], P('ep'), may hold values from 0.05 to 1
- norm_gain: float32 [2048], replicated, may hold values from 0.1 to 1.9
- w_gate: bfloat16 [64, 2048, 2048], P('ep', None, 'tp'), may hold values from -0.33007812 to 0.33007812
- w_up: bfloat16 [64, 2048, 2048], P('ep', None, 'tp'), may hold values from -0.33007812 to 0.33007812
- w_down: bfloat16 [64, 2048, 2048], P('ep', 'tp'), may hold values from -0.026489258 to 0.026489258
Outputs:
- mixed: bfloat16 [1024, 2048], P('ep', 'tp')
Inputs may be any that keep to these rules, and one draw needn't show every extreme that they name: `routing`: each token names 4 different experts. Among the 32 tokens of one index of ep no expert is named more than 8 times, a bound that some block reaches.
All inputs are finite; a program needn't handle non-finite values.
Results may differ from a plain program's by a relative error of at most 0.015.
Values may be sent and summed in bfloat16 or wider, within the bound.
A program may use at most 128 MiB of HBM per device.

v0:
```python
import functools

import jax
import jax.numpy as jnp
from jax import lax
from jax.experimental import pallas as pl
from jax.experimental.pallas import tpu as pltpu
from jax.sharding import PartitionSpec as P

CAP = 8
MESH = pl.DeviceIdType.MESH

norm_eps = 1e-06
clamp_limit = 7.0
swish_alpha = 1.702


def partner(me, step, n):
    if n & (n - 1):
        return lax.rem(me + step, n)
    other, bit = 0, 1
    while bit < n:
        mine = (me // bit) % 2
        other = other + bit * ((1 - mine) if step & bit else mine)
        bit *= 2
    return other


def kernel(
    n_ep,
    n_tp,
    tok_hbm,
    rout_hbm,
    gw_hbm,
    gain_hbm,
    wg_hbm,
    wu_hbm,
    wd_hbm,
    out_ref,
    tok_ref,
    rout_ref,
    gw_ref,
    gain_ref,
    wg,
    wu,
    wd,
    outgoing,
    rows,
    combine,
    acc_gate,
    acc_up,
    part,
    part_in,
    ret_out,
    ret_in,
    in_sem,
    w_sem,
    disp_send,
    disp_recv,
    gath_send,
    gath_recv,
    part_send,
    part_recv,
    ret_send,
    ret_recv,
):
    ep, tp = lax.axis_index("ep"), lax.axis_index("tp")
    n_exp, width, ff = wg_hbm.shape
    n_tok, cols = tok_ref.shape
    top = rout_ref.shape[0]
    chunk = n_exp * CAP
    slots = n_ep * chunk

    small = [
        pltpu.make_async_copy(src, dst, in_sem.at[i])
        for i, (src, dst) in enumerate(
            ((rout_hbm, rout_ref), (gw_hbm, gw_ref), (tok_hbm, tok_ref), (gain_hbm, gain_ref))
        )
    ]
    for copy in small:
        copy.start()

    barrier = pltpu.get_barrier_semaphore()
    for step in range(1, n_ep):
        pl.semaphore_signal(
            barrier, inc=1, device_id=(partner(ep, step, n_ep), tp), device_id_type=MESH
        )
    for step in range(1, n_tp):
        pl.semaphore_signal(
            barrier, inc=1, device_id=(ep, partner(tp, step, n_tp)), device_id_type=MESH
        )

    loads = []
    for e in range(n_exp):
        for i, (src, dst) in enumerate(((wg_hbm, wg), (wu_hbm, wu), (wd_hbm, wd))):
            loads.append(pltpu.make_async_copy(src.at[e], dst.at[e], w_sem.at[i, e]))
    order = [3 * e + i for e in range(n_exp) for i in (0, 1)] + [3 * e + 2 for e in range(n_exp)]
    for at in order:
        loads[at].start()

    slot = lax.broadcasted_iota(jnp.int32, (slots, n_tok), 0)
    slot_exp, slot_rank = slot // CAP, slot % CAP
    named = jnp.zeros((slots, n_tok), jnp.float32)
    weight = jnp.zeros((slots, n_tok), jnp.float32)
    small[0].wait()
    small[1].wait()
    for k in range(top):
        hit = rout_ref[k : k + 1, :] == slot_exp
        named = named + jnp.where(hit, 1.0, 0.0)
        weight = weight + jnp.where(hit, gw_ref[k : k + 1, :], 0.0)
    earlier = jnp.where(
        lax.broadcasted_iota(jnp.int32, (n_tok, n_tok), 0)
        < lax.broadcasted_iota(jnp.int32, (n_tok, n_tok), 1),
        1.0,
        0.0,
    ).astype(jnp.bfloat16)
    rank = jnp.dot(named.astype(jnp.bfloat16), earlier, preferred_element_type=jnp.float32)
    placing = jnp.where(rank == slot_rank.astype(jnp.float32), named, 0.0)
    small[2].wait()
    sent = jnp.dot(
        placing.astype(jnp.bfloat16), tok_ref[...], preferred_element_type=jnp.float32
    )
    outgoing[...] = sent.astype(jnp.bfloat16).reshape(n_ep, chunk, cols)
    rows[tp, ep] = outgoing[ep]

    pl.semaphore_wait(barrier, n_ep - 1 + n_tp - 1)

    def dispatch(peer, slot):
        return pltpu.make_async_remote_copy(
            src_ref=outgoing.at[peer],
            dst_ref=rows.at[tp, slot],
            send_sem=disp_send.at[peer],
            recv_sem=disp_recv.at[slot],
            device_id=(peer, tp),
            device_id_type=MESH,
        )

    def gather(src, peer, source_tp, s):
        return pltpu.make_async_remote_copy(
            src_ref=src,
            dst_ref=rows.at[source_tp, s],
            send_sem=gath_send.at[peer, s],
            recv_sem=gath_recv.at[source_tp, s],
            device_id=(ep, peer),
            device_id_type=MESH,
        )

    def reduce(peer, slot, e):
        return pltpu.make_async_remote_copy(
            src_ref=part.at[peer, e],
            dst_ref=part_in.at[slot, e],
            send_sem=part_send.at[peer, e],
            recv_sem=part_recv.at[slot, e],
            device_id=(ep, peer),
            device_id_type=MESH,
        )

    def give_back(peer, slot, e):
        return pltpu.make_async_remote_copy(
            src_ref=ret_out.at[e, peer],
            dst_ref=ret_in.at[e, slot],
            send_sem=ret_send.at[e, peer],
            recv_sem=ret_recv.at[e, slot],
            device_id=(peer, tp),
            device_id_type=MESH,
        )

    def finish(pre_gate, pre_up, factor, e):
        clamped = jnp.minimum(pre_gate * factor, clamp_limit)
        upper = jnp.clip(pre_up * factor, -clamp_limit, clamp_limit)
        hidden = (clamped * jax.nn.sigmoid(swish_alpha * clamped) * (upper + 1.0)).astype(
            jnp.bfloat16
        )
        loads[3 * e + 2].wait()
        for hop in reversed(range(n_tp)):
            q = partner(tp, hop, n_tp) if hop else tp
            at = pl.multiple_of(q * cols, cols)
            part[q, e] = jnp.dot(
                hidden, wd[e, :, pl.ds(at, cols)], preferred_element_type=jnp.float32
            ).astype(jnp.bfloat16)
            if hop:
                reduce(q, tp, e).start()

    for step in reversed(range(1, n_ep)):
        dispatch(partner(ep, step, n_ep), ep).start()
    for step in range(1, n_tp):
        gather(outgoing.at[ep], partner(tp, step, n_tp), tp, ep).start()
    for step in range(1, n_ep):
        s = partner(ep, step, n_ep)
        dispatch(s, s).wait_recv()
        for hop in range(1, n_tp):
            gather(rows.at[tp, s], partner(tp, hop, n_tp), tp, s).start()

    combine[...] = (placing * weight).T
    small[3].wait()

    ssq = jnp.zeros((n_ep, chunk, 1), jnp.float32)
    for hop in range(n_tp):
        j = partner(tp, hop, n_tp) if hop else tp
        if hop:
            for s in range(n_ep):
                gather(rows.at[tp, s], j, j, s).wait_recv()
        at = pl.multiple_of(j * cols, cols)
        wide = rows[j].astype(jnp.float32)
        ssq = ssq + jnp.sum(wide * wide, axis=2, keepdims=True)
        scaled = (wide * gain_ref[:, pl.ds(at, cols)].reshape(1, 1, cols)).reshape(
            n_ep, n_exp, CAP, cols
        )
        if hop == n_tp - 1:
            scale = lax.rsqrt(ssq / width + norm_eps).reshape(n_ep, n_exp, CAP, 1)
        for e in range(n_exp):
            x = scaled[:, e].reshape(n_ep * CAP, cols).astype(jnp.bfloat16)
            pre = []
            for i, (w, acc) in enumerate(((wg, acc_gate), (wu, acc_up))):
                if hop == 0:
                    loads[3 * e + i].wait()
                y = jnp.dot(x, w[e, pl.ds(at, cols), :], preferred_element_type=jnp.float32)
                if hop:
                    y = acc[e] + y
                if hop < n_tp - 1:
                    acc[e] = y
                pre.append(y)
            if hop == n_tp - 1:
                finish(pre[0], pre[1], scale[:, e].reshape(n_ep * CAP, 1), e)

    for e in range(n_exp):
        total = part[tp, e].astype(jnp.float32)
        for hop in range(1, n_tp):
            j = partner(tp, hop, n_tp)
            reduce(j, j, e).wait_recv()
            total = total + part_in[j, e].astype(jnp.float32)
        ret_out[e] = total.reshape(n_ep, CAP, cols).astype(jnp.bfloat16)
        for step in reversed(range(1, n_ep)):
            give_back(partner(ep, step, n_ep), ep, e).start()
        ret_in[e, ep] = ret_out[e, ep]

    both = combine[...]
    high = both.astype(jnp.bfloat16)
    low = (both - high.astype(jnp.float32)).astype(jnp.bfloat16)

    for step in range(1, n_ep):
        dispatch(partner(ep, step, n_ep), ep).wait_send()
    for hop in range(1, n_tp):
        q = partner(tp, hop, n_tp)
        for s in range(n_ep):
            gather(rows.at[tp, s], q, tp, s).wait_send()
        for e in range(n_exp):
            reduce(q, tp, e).wait_send()
    for e in range(n_exp):
        for step in range(1, n_ep):
            s = partner(ep, step, n_ep)
            give_back(s, s, e).wait_recv()
    back = jnp.stack([ret_in[e].astype(jnp.float32) for e in range(n_exp)], axis=1)
    back = back.reshape(slots, cols).astype(jnp.bfloat16)
    out_ref[...] = (
        jnp.dot(high, back, preferred_element_type=jnp.float32)
        + jnp.dot(low, back, preferred_element_type=jnp.float32)
    ).astype(jnp.bfloat16)
    for e in range(n_exp):
        for step in range(1, n_ep):
            give_back(partner(ep, step, n_ep), ep, e).wait_send()


def per_device(tokens, routing, gate_weights, norm_gain, w_gate, w_up, w_down):
    n_ep, n_tp = lax.axis_size("ep"), lax.axis_size("tp")
    n_exp, width, ff = w_gate.shape
    n_tok, cols = tokens.shape
    chunk = n_exp * CAP
    slots = n_ep * chunk
    vmem = pl.BlockSpec(memory_space=pltpu.VMEM)
    hbm = pl.BlockSpec(memory_space=pltpu.HBM)
    bf16, f32 = jnp.bfloat16, jnp.float32
    dma = pltpu.SemaphoreType.DMA
    return pl.pallas_call(
        functools.partial(kernel, n_ep, n_tp),
        out_shape=jax.ShapeDtypeStruct((n_tok, cols), bf16),
        in_specs=[hbm] * 7,
        out_specs=vmem,
        scratch_shapes=[
            pltpu.VMEM(tokens.shape, bf16),
            pltpu.VMEM(routing.shape[::-1], jnp.int32),
            pltpu.VMEM(gate_weights.shape[::-1], f32),
            pltpu.VMEM((1, width), f32),
            pltpu.VMEM(w_gate.shape, bf16),
            pltpu.VMEM(w_up.shape, bf16),
            pltpu.VMEM(w_down.shape, bf16),
            pltpu.VMEM((n_ep, chunk, cols), bf16),
            pltpu.VMEM((n_tp, n_ep, chunk, cols), bf16),
            pltpu.VMEM((n_tok, slots), f32),
            pltpu.VMEM((n_exp, n_ep * CAP, ff), f32),
            pltpu.VMEM((n_exp, n_ep * CAP, ff), f32),
            pltpu.VMEM((n_tp, n_exp, n_ep * CAP, cols), bf16),
            pltpu.VMEM((n_tp, n_exp, n_ep * CAP, cols), bf16),
            pltpu.VMEM((n_exp, n_ep, CAP, cols), bf16),
            pltpu.VMEM((n_exp, n_ep, CAP, cols), bf16),
            dma((4,)),
            dma((3, n_exp)),
            dma((n_ep,)),
            dma((n_ep,)),
            dma((n_tp, n_ep)),
            dma((n_tp, n_ep)),
            dma((n_tp, n_exp)),
            dma((n_tp, n_exp)),
            dma((n_exp, n_ep)),
            dma((n_exp, n_ep)),
        ],
        compiler_params=pltpu.CompilerParams(collective_id=0, has_side_effects=True),
    )(tokens, routing.T, gate_weights.T, norm_gain.reshape(1, width), w_gate, w_up, w_down)


def solution(mesh):
    in_specs = (
        P("ep", "tp"),
        P("ep", None),
        P("ep", None),
        P(),
        P("ep", None, "tp"),
        P("ep", None, "tp"),
        P("ep", "tp", None),
    )
    return jax.shard_map(
        per_device, mesh=mesh, in_specs=in_specs, out_specs=P("ep", "tp"), check_vma=False
    )
```

profile of v0, /device:TPU:1, one launch (start us, length us, event | category | flops | bytes accessed | tf_op | source)
XLA Modules:
  0.0 100.2 jit_solution(7804283137654638740)
XLA Ops:
  0.0 98.9 %shard_map.73 = bf16[32,128]{1,0:T(8,128)(2,1)} custom-call(bf16[32,128]{1,0:T(8,128)(2,1)} %tok_hbm.1, s32[4,32]{1,0:T(4,128)} %bitcast.4, f32[4,32]{1,0:T(4,128)} %bitcast.5, f32[1,2048]{1,0:T(1,128)} %bitcast.3, bf16[2,2048,128]{2,1,0:T(8,128)(2,1)} %wg_hbm.1, bf16[2,2048,128]{2,1,0:T(8,128)(2,1)} %wu_hbm.1, bf16[2,128,2048]{2,1,0:T(8,128)(2,1)} %wd_hbm.1), custom_call_target="tpu_custom_call" | custom-call | tf_op jit(solution)/shard_map/pallas_call | solution.py:274
  98.9 1.3 %copy.9 = bf16[32,128]{1,0:T(8,128)(2,1)} copy(bf16[32,128]{1,0:T(8,128)(2,1)} %shard_map.73) | data formatting | bytes 16384
where the time goes:
time: 100 us
  Pallas kernels  98.9 us (99%)
  local copies, waits for them, and re-layouts  1.3 us (1%)
    pallas_call x1, Pallas kernels, per_device(): pl.pallas_call(functools.partial(kernel, n_ep, n_tp), out_shape=jax.Shape...  98.9 us

commit v1 on v0

v1 whole, which is shorter than its diff:
```python
import functools

import jax
import jax.numpy as jnp
from jax import lax
from jax.experimental import pallas as pl
from jax.experimental.pallas import tpu as pltpu
from jax.sharding import PartitionSpec as P

CAP = 8
SIDE = 4
CORES = 2
PER = 4
FORWARD = False
DZS = (0, 1, -1, 2, 8, 7, -7, 6, -6, 5, -5, 4, -4, 3, -3, -2)
PLAN = ((7, 0), (7, 1), (0, 0), (7, 2), (0, 1), (1, 0), (7, 3), (0, 7), (0, 6), (1, 1), (1, 6), (3, 0), (1, 7), (0, 2), (0, 3), (0, 5), (0, 4), (3, 1), (3, 6), (3, 7), (1, 2), (1, 4), (5, 0), (1, 3), (1, 5), (5, 1), (5, 6), (5, 7), (6, 0), (3, 2), (3, 3), (3, 4), (6, 1), (6, 7), (3, 5), (6, 6), (5, 2), (5, 3), (5, 4), (5, 5), (6, 3), (6, 2), (6, 4), (6, 5))
COMBINE_AT = 6
MESH = pl.DeviceIdType.MESH

norm_eps = 1e-06
clamp_limit = 7.0
swish_alpha = 1.702


def arrangement(n_z):
    return [(dz % n_z, dc) for dz in DZS for dc in range(CORES)]


def kernel(
    n_ep,
    n_tp,
    tok_hbm,
    rout_hbm,
    gw_hbm,
    gain_hbm,
    wg_hbm,
    wu_hbm,
    wd_hbm,
    out_ref,
    tok_ref,
    rout_ref,
    gw_ref,
    gain_ref,
    wgu,
    wd,
    outgoing,
    rows,
    combine,
    part,
    far_in,
    near_in,
    light_in,
    ret_out,
    ret_in,
    in_sem,
    w_sem,
    disp_send,
    disp_recv,
    a_send,
    a_recv,
    b_send,
    b_recv,
    c_send,
    c_recv,
    far_send,
    far_recv,
    near_send,
    near_recv,
    light_send,
    light_recv,
    ret_send,
    ret_recv,
    open_sem,
):
    ep, tp = lax.axis_index("ep"), lax.axis_index("tp")
    n_exp, width, ff = wg_hbm.shape
    n_tok, cols = tok_ref.shape
    top = rout_ref.shape[0]
    chunk = n_exp * CAP
    slots = n_ep * chunk
    n_z = n_ep // CORES
    order = arrangement(n_z)
    groups = n_ep // PER
    block = PER * chunk
    z, core = ep // CORES, ep % CORES
    y, x = tp // SIDE, tp % SIDE

    def owner(p):
        dz, dc = order[p]
        return lax.rem(z + dz, n_z) * CORES + (1 - core if dc else core)

    def mirror(p):
        dz, dc = order[p]
        return order.index(((n_z - dz) % n_z, dc))

    def at(yy, xx):
        return lax.rem(yy, SIDE) * SIDE + lax.rem(xx, SIDE)

    small = [
        pltpu.make_async_copy(src, dst, in_sem.at[i])
        for i, (src, dst) in enumerate(
            ((rout_hbm, rout_ref), (gw_hbm, gw_ref), (tok_hbm, tok_ref), (gain_hbm, gain_ref))
        )
    ]
    for copy in small:
        copy.start()

    barrier = pltpu.get_barrier_semaphore()
    def reach(p):
        dz = order[p][0]
        return min(dz, n_z - dz)

    near = [p for p in range(1, n_ep) if reach(p) <= 1]
    for p in near:
        pl.semaphore_signal(barrier, inc=1, device_id=(owner(p), tp), device_id_type=MESH)
    for step in range(1, SIDE):
        pl.semaphore_signal(barrier, inc=1, device_id=(ep, at(y, x + step)), device_id_type=MESH)
        pl.semaphore_signal(barrier, inc=1, device_id=(ep, at(y + step, x)), device_id_type=MESH)

    loads = []
    for e in range(n_exp):
        for i, (src, dst) in enumerate(
            (
                (wg_hbm.at[e], wgu.at[e, :, pl.ds(0, ff)]),
                (wu_hbm.at[e], wgu.at[e, :, pl.ds(ff, ff)]),
                (wd_hbm.at[e], wd.at[e]),
            )
        ):
            loads.append(pltpu.make_async_copy(src, dst, w_sem.at[i, e]))
    for load in loads:
        load.start()

    slot_exp = jnp.concatenate(
        [
            owner(p) * n_exp + lax.broadcasted_iota(jnp.int32, (chunk, n_tok), 0) // CAP
            for p in range(n_ep)
        ],
        axis=0,
    )
    slot_rank = lax.broadcasted_iota(jnp.int32, (slots, n_tok), 0) % CAP
    named = jnp.zeros((slots, n_tok), jnp.float32)
    weight = jnp.zeros((slots, n_tok), jnp.float32)
    small[0].wait()
    small[1].wait()
    for k in range(top):
        hit = rout_ref[k : k + 1, :] == slot_exp
        named = named + jnp.where(hit, 1.0, 0.0)
        weight = weight + jnp.where(hit, gw_ref[k : k + 1, :], 0.0)
    earlier = jnp.where(
        lax.broadcasted_iota(jnp.int32, (n_tok, n_tok), 0)
        < lax.broadcasted_iota(jnp.int32, (n_tok, n_tok), 1),
        1.0,
        0.0,
    ).astype(jnp.bfloat16)
    rank = jnp.dot(named.astype(jnp.bfloat16), earlier, preferred_element_type=jnp.float32)
    placing = jnp.where(rank == slot_rank.astype(jnp.float32), named, 0.0)
    small[2].wait()
    sent = jnp.dot(
        placing.astype(jnp.bfloat16), tok_ref[...], preferred_element_type=jnp.float32
    ).astype(jnp.bfloat16)
    outgoing[...] = sent.reshape(n_ep, chunk, cols)
    rows[0, y, x, 0:chunk] = outgoing[0]


    def remote(src, dst, send, recv, peer):
        return pltpu.make_async_remote_copy(
            src_ref=src,
            dst_ref=dst,
            send_sem=send,
            recv_sem=recv,
            device_id=peer,
            device_id_type=MESH,
        )

    def dispatch(p, slot):
        g, s = divmod(slot, PER)
        return remote(
            outgoing.at[p],
            rows.at[g, y, x, pl.ds(s * chunk, chunk)],
            disp_send.at[p],
            disp_recv.at[slot],
            (owner(p), tp),
        )

    def heavy_y(g):
        return g % 2 == 0

    def place(g):
        return (y, x) if heavy_y(g) else (x, y)

    def peer(g, heavy, light):
        return (ep, at(heavy, light) if heavy_y(g) else at(light, heavy))

    def one(ref, g, heavy, light):
        heavy, light = lax.rem(heavy, SIDE), lax.rem(light, SIDE)
        return ref.at[g, heavy, light] if heavy_y(g) else ref.at[g, light, heavy]

    def line(ref, g, heavy, start=0, size=SIDE):
        heavy = lax.rem(heavy, SIDE)
        if heavy_y(g):
            return ref.at[g, heavy, pl.ds(start, size)]
        return ref.at[g, pl.ds(start, size), heavy]

    half = SIDE // 2
    steps = (1, SIDE - 1, 2)
    ways = (1, SIDE - 1) if FORWARD else steps
    n_ways = len(ways)

    def along_light(g, k):
        h, l = place(g)
        ref = one(rows, g, h, l)
        return remote(ref, ref, a_send.at[g, k], a_recv.at[g, k], peer(g, h, l + steps[k]))

    def along_heavy(g, k):
        h, l = place(g)
        ref = line(rows, g, h)
        return remote(ref, ref, b_send.at[g, k], b_recv.at[g, k], peer(g, h + ways[k], l))

    def pass_on(g, k):
        h, l = place(g)
        ref = line(rows, g, h + SIDE - ways[k], k * half, half)
        return remote(ref, ref, c_send.at[g, k], c_recv.at[g, k], peer(g, h + ways[k], l))

    def far_part(g, k):
        h, l = place(g)
        return remote(
            line(part, g, h + 2, k * half, half),
            far_in.at[g, k],
            far_send.at[g, k],
            far_recv.at[g, k],
            peer(g, h + ways[k], l),
        )

    def near_part(g, k, which):
        h, l = place(g)
        return remote(
            line(part, g, h + ways[k], which * half, half),
            near_in.at[g, k, pl.ds(which * half, half)],
            near_send.at[g, k, which],
            near_recv.at[g, k, which],
            peer(g, h + ways[k], l),
        )

    def whole_part(g, k):
        h, l = place(g)
        return remote(
            line(part, g, h + ways[k]),
            near_in.at[g, k],
            near_send.at[g, k, 0],
            near_recv.at[g, k, 0],
            peer(g, h + ways[k], l),
        )

    def light_part(g, k):
        h, l = place(g)
        return remote(
            one(part, g, h, l + steps[k]),
            light_in.at[g, k],
            light_send.at[g, k],
            light_recv.at[g, k],
            peer(g, h, l + steps[k]),
        )

    def give_back(p, slot):
        return remote(
            ret_out.at[p], ret_in.at[slot], ret_send.at[p], ret_recv.at[slot], (owner(p), tp)
        )

    hops = (1, 2, 4)

    def stage_open(k):
        if k == 0:
            pl.semaphore_wait(barrier, len(near) + 2 * (SIDE - 1))
        else:
            pl.semaphore_wait(open_sem.at[k - 1], 2)
        if k < len(hops):
            for d in (hops[k], n_z - hops[k]):
                pl.semaphore_signal(
                    open_sem.at[k],
                    inc=1,
                    device_id=(lax.rem(z + d, n_z) * CORES + core, tp),
                    device_id_type=MESH,
                )
        least = hops[k - 1] + 1 if k else 0
        most = 2 * least - 2 if k else 1
        for p in range(1, n_ep):
            if least <= reach(p) <= most:
                dispatch(p, mirror(p)).start()

    def stage_take(g):
        for p in range(g * PER, (g + 1) * PER):
            if p:
                dispatch(p, p).wait_recv()
        for k in range(3):
            along_light(g, k).start()

    def stage_spread(g):
        for k in range(3):
            along_light(g, k).wait_recv()
        for k in range(n_ways):
            along_heavy(g, k).start()

    def stage_pass(g):
        for k in range(2):
            along_heavy(g, k).wait_recv()
            pass_on(g, k).start()

    def stage_compute(g):
        if FORWARD:
            for k in range(2):
                pass_on(g, k).wait_recv()
        else:
            for k in range(n_ways):
                along_heavy(g, k).wait_recv()
        if g == 0:
            small[3].wait()
        ssq = jnp.zeros((block, cols), jnp.float32)
        xs = [[] for _ in range(n_exp)]
        for j in range(n_tp):
            wide = rows[g, j // SIDE, j % SIDE].astype(jnp.float32)
            ssq = ssq + wide * wide
            scaled = (wide * gain_ref[:, j * cols : (j + 1) * cols]).reshape(
                PER, n_exp, CAP, cols
            )
            for e in range(n_exp):
                xs[e].append(scaled[:, e].reshape(PER * CAP, cols).astype(jnp.bfloat16))
        total = jnp.sum(ssq, axis=1, keepdims=True)
        scale = lax.rsqrt(total / width + norm_eps).reshape(PER, n_exp, CAP, 1)
        for e in range(n_exp):
            if g == 0:
                for i in range(3):
                    loads[3 * e + i].wait()
            pre = jnp.dot(
                jnp.concatenate(xs[e], axis=1), wgu[e], preferred_element_type=jnp.float32
            )
            pre = pre * scale[:, e].reshape(PER * CAP, 1)
            clamped = jnp.minimum(pre[:, :ff], clamp_limit)
            upper = jnp.clip(pre[:, ff:], -clamp_limit, clamp_limit)
            hidden = (clamped * jax.nn.sigmoid(swish_alpha * clamped) * (upper + 1.0)).astype(
                jnp.bfloat16
            )
            down = jnp.dot(hidden, wd[e], preferred_element_type=jnp.float32).astype(
                jnp.bfloat16
            )
            for q in range(n_tp):
                part[g, q // SIDE, q % SIDE, e * PER * CAP : (e + 1) * PER * CAP] = down[
                    :, q * cols : (q + 1) * cols
                ]
        if FORWARD:
            for k in range(2):
                far_part(g, k).start()
                near_part(g, k, 1 - k).start()
        else:
            for k in range(n_ways):
                whole_part(g, k).start()

    def stage_join(g):
        h, l = place(g)
        for k in range(2):
            far_part(g, k).wait_recv()
            mine = line(part, g, h + ways[k], k * half, half)
            mine[...] = (
                mine[...].astype(jnp.float32) + far_in[g, k].astype(jnp.float32)
            ).astype(jnp.bfloat16)
            near_part(g, k, k).start()

    def stage_sum(g):
        h, l = place(g)
        mine = line(part, g, h)
        total = mine[...].astype(jnp.float32)
        for k in range(n_ways):
            if FORWARD:
                for which in range(2):
                    near_part(g, k, which).wait_recv()
            else:
                whole_part(g, k).wait_recv()
            total = total + near_in[g, k].astype(jnp.float32)
        mine[...] = total.astype(jnp.bfloat16)
        for k in range(3):
            light_part(g, k).start()

    def stage_return(g):
        h, l = place(g)
        total = one(part, g, h, l)[...].astype(jnp.float32)
        for k in range(3):
            light_part(g, k).wait_recv()
            total = total + light_in[g, k].astype(jnp.float32)
        total = total.reshape(n_exp, PER, CAP, cols)
        back = jnp.stack([total[e] for e in range(n_exp)], axis=1).reshape(PER, chunk, cols)
        ret_out[g * PER : (g + 1) * PER] = back.astype(jnp.bfloat16)
        for p in range(g * PER, (g + 1) * PER):
            if p:
                give_back(p, mirror(p)).start()
            else:
                ret_in[0] = ret_out[0]


    stages = (
        stage_take,
        stage_spread,
        stage_pass,
        stage_compute,
        stage_join,
        stage_sum,
        stage_return,
        stage_open,
    )
    for step, (stage, g) in enumerate(PLAN):
        stages[stage](g)
        if step == COMBINE_AT:
            combine[...] = (placing * weight).T

    both = combine[...]
    high = both.astype(jnp.bfloat16)
    low = (both - high.astype(jnp.float32)).astype(jnp.bfloat16)

    for p in range(1, n_ep):
        dispatch(p, mirror(p)).wait_send()
    for g in range(groups):
        for k in range(3):
            along_light(g, k).wait_send()
            light_part(g, k).wait_send()
        for k in range(n_ways):
            along_heavy(g, k).wait_send()
            if FORWARD:
                pass_on(g, k).wait_send()
                far_part(g, k).wait_send()
                for which in range(2):
                    near_part(g, k, which).wait_send()
            else:
                whole_part(g, k).wait_send()
    for p in range(1, n_ep):
        give_back(p, p).wait_recv()
    back = ret_in[...].reshape(slots, cols)
    out_ref[...] = (
        jnp.dot(high, back, preferred_element_type=jnp.float32)
        + jnp.dot(low, back, preferred_element_type=jnp.float32)
    ).astype(jnp.bfloat16)
    for p in range(1, n_ep):
        give_back(p, mirror(p)).wait_send()


def per_device(tokens, routing, gate_weights, norm_gain, w_gate, w_up, w_down):
    n_ep, n_tp = lax.axis_size("ep"), lax.axis_size("tp")
    n_exp, width, ff = w_gate.shape
    n_tok, cols = tokens.shape
    chunk = n_exp * CAP
    slots = n_ep * chunk
    groups, block = n_ep // PER, PER * chunk
    vmem = pl.BlockSpec(memory_space=pltpu.VMEM)
    hbm = pl.BlockSpec(memory_space=pltpu.HBM)
    bf16, f32 = jnp.bfloat16, jnp.float32
    dma = pltpu.SemaphoreType.DMA
    return pl.pallas_call(
        functools.partial(kernel, n_ep, n_tp),
        out_shape=jax.ShapeDtypeStruct((n_tok, cols), bf16),
        in_specs=[hbm] * 7,
        out_specs=vmem,
        scratch_shapes=[
            pltpu.VMEM(tokens.shape, bf16),
            pltpu.VMEM(routing.shape[::-1], jnp.int32),
            pltpu.VMEM(gate_weights.shape[::-1], f32),
            pltpu.VMEM((1, width), f32),
            pltpu.VMEM((n_exp, width, 2 * ff), bf16),
            pltpu.VMEM(w_down.shape, bf16),
            pltpu.VMEM((n_ep, chunk, cols), bf16),
            pltpu.VMEM((groups, SIDE, SIDE, block, cols), bf16),
            pltpu.VMEM((n_tok, slots), f32),
            pltpu.VMEM((groups, SIDE, SIDE, block, cols), bf16),
            pltpu.VMEM((groups, 2, SIDE // 2, block, cols), bf16),
            pltpu.VMEM((groups, 3, SIDE, block, cols), bf16),
            pltpu.VMEM((groups, 3, block, cols), bf16),
            pltpu.VMEM((n_ep, chunk, cols), bf16),
            pltpu.VMEM((n_ep, chunk, cols), bf16),
            dma((4,)),
            dma((3, n_exp)),
            dma((n_ep,)),
            dma((n_ep,)),
            dma((groups, 3)),
            dma((groups, 3)),
            dma((groups, 3)),
            dma((groups, 3)),
            dma((groups, 2)),
            dma((groups, 2)),
            dma((groups, 2)),
            dma((groups, 2)),
            dma((groups, 3, 2)),
            dma((groups, 3, 2)),
            dma((groups, 3)),
            dma((groups, 3)),
            dma((n_ep,)),
            dma((n_ep,)),
            pltpu.SemaphoreType.REGULAR((3,)),
        ],
        compiler_params=pltpu.CompilerParams(collective_id=0, has_side_effects=True),
    )(tokens, routing.T, gate_weights.T, norm_gain.reshape(1, width), w_gate, w_up, w_down)


def solution(mesh):
    in_specs = (
        P("ep", "tp"),
        P("ep", None),
        P("ep", None),
        P(),
        P("ep", None, "tp"),
        P("ep", None, "tp"),
        P("ep", "tp", None),
    )
    return jax.shard_map(
        per_device, mesh=mesh, in_specs=in_specs, out_specs=P("ep", "tp"), check_vma=False
    )
```

time: 100 us -> 68.4 us (0.68)
  Pallas kernels: 98.9 us -> 66.9 us
    pallas_call x1, Pallas kernels: 98.9 us -> 66.9 us  [per_device(): pl.pallas_call(functools.partial(kernel, n_ep, n_tp), out_shape=jax.Shape...]
where the time goes in v1:
time: 68.4 us; the launch traced here: 68.2 us
  Pallas kernels  66.9 us (98%)
  local copies, waits for them, and re-layouts  1.3 us (2%)
    pallas_call x1, Pallas kernels, per_device(): pl.pallas_call(functools.partial(kernel, n_ep, n_tp), out_shape=jax.Shape...  66.9 us

profile of v1, /device:TPU:1, one launch (start us, length us, event | category | flops | bytes accessed | tf_op | source)
XLA Modules:
  0.0 68.2 jit_solution(2684030671697891211)
XLA Ops:
  0.0 66.9 %shard_map.73 = bf16[32,128]{1,0:T(8,128)(2,1)} custom-call(bf16[32,128]{1,0:T(8,128)(2,1)} %tok_hbm.1, s32[4,32]{1,0:T(4,128)} %bitcast.4, f32[4,32]{1,0:T(4,128)} %bitcast.5, f32[1,2048]{1,0:T(1,128)} %bitcast.3, bf16[2,2048,128]{2,1,0:T(8,128)(2,1)} %wg_hbm.1, bf16[2,2048,128]{2,1,0:T(8,128)(2,1)} %wu_hbm.1, bf16[2,128,2048]{2,1,0:T(8,128)(2,1)} %wd_hbm.1), custom_call_target="tpu_custom_call" | custom-call | tf_op jit(solution)/shard_map/pallas_call | solution.py:454
  66.9 1.3 %copy.9 = bf16[32,128]{1,0:T(8,128)(2,1)} copy(bf16[32,128]{1,0:T(8,128)(2,1)} %shard_map.73) | data formatting | bytes 16384

commit v2 on v1

--- a/solution.py
+++ b/solution.py
@@ -11,9 +11,8 @@
 SIDE = 4
 CORES = 2
 PER = 4
-FORWARD = False
-DZS = (0, 1, -1, 2, 8, 7, -7, 6, -6, 5, -5, 4, -4, 3, -3, -2)
-PLAN = ((7, 0), (7, 1), (0, 0), (7, 2), (0, 1), (1, 0), (7, 3), (0, 7), (0, 6), (1, 1), (1, 6), (3, 0), (1, 7), (0, 2), (0, 3), (0, 5), (0, 4), (3, 1), (3, 6), (3, 7), (1, 2), (1, 4), (5, 0), (1, 3), (1, 5), (5, 1), (5, 6), (5, 7), (6, 0), (3, 2), (3, 3), (3, 4), (6, 1), (6, 7), (3, 5), (6, 6), (5, 2), (5, 3), (5, 4), (5, 5), (6, 3), (6, 2), (6, 4), (6, 5))
+DZS = (0, 1, -1, 2, -2, 3, -3, 4, 8, 7, -7, 6, -6, 5, -5, -4)
+PLAN = ((0, 0), (0, 1), (0, 2), (0, 3), (1, 0), (0, 7), (0, 6), (0, 5), (1, 1), (0, 4), (1, 2), (1, 3), (2, 0), (1, 6), (2, 1), (1, 7), (1, 5), (1, 4), (2, 2), (2, 3), (3, 0), (3, 1), (2, 6), (2, 7), (2, 4), (2, 5), (3, 2), (3, 3), (4, 0), (4, 1), (3, 6), (3, 7), (3, 4), (3, 5), (4, 2), (4, 3), (5, 0), (5, 1), (4, 6), (4, 7), (4, 4), (4, 5), (5, 2), (5, 3), (6, 1), (5, 6), (6, 0), (5, 7), (5, 4), (5, 5), (6, 2), (6, 3), (6, 6), (6, 7), (6, 4), (6, 5))
 COMBINE_AT = 6
 MESH = pl.DeviceIdType.MESH
 
@@ -70,7 +69,6 @@
     light_recv,
     ret_send,
     ret_recv,
-    open_sem,
 ):
     ep, tp = lax.axis_index("ep"), lax.axis_index("tp")
     n_exp, width, ff = wg_hbm.shape
@@ -106,12 +104,7 @@
         copy.start()
 
     barrier = pltpu.get_barrier_semaphore()
-    def reach(p):
-        dz = order[p][0]
-        return min(dz, n_z - dz)
-
-    near = [p for p in range(1, n_ep) if reach(p) <= 1]
-    for p in near:
+    for p in reversed(range(1, n_ep)):
         pl.semaphore_signal(barrier, inc=1, device_id=(owner(p), tp), device_id_type=MESH)
     for step in range(1, SIDE):
         pl.semaphore_signal(barrier, inc=1, device_id=(ep, at(y, x + step)), device_id_type=MESH)
@@ -130,22 +123,20 @@
     for load in loads:
         load.start()
 
+    which = jnp.concatenate([jnp.full((CAP, n_tok), e, jnp.int32) for e in range(n_exp)], axis=0)
     slot_exp = jnp.concatenate(
         [
-            owner(p) * n_exp + lax.broadcasted_iota(jnp.int32, (chunk, n_tok), 0) // CAP
+            owner(p) * n_exp + which
             for p in range(n_ep)
         ],
         axis=0,
     )
-    slot_rank = lax.broadcasted_iota(jnp.int32, (slots, n_tok), 0) % CAP
+    slot_rank = lax.broadcasted_iota(jnp.int32, (slots, n_tok), 0) & (CAP - 1)
     named = jnp.zeros((slots, n_tok), jnp.float32)
-    weight = jnp.zeros((slots, n_tok), jnp.float32)
     small[0].wait()
-    small[1].wait()
     for k in range(top):
         hit = rout_ref[k : k + 1, :] == slot_exp
         named = named + jnp.where(hit, 1.0, 0.0)
-        weight = weight + jnp.where(hit, gw_ref[k : k + 1, :], 0.0)
     earlier = jnp.where(
         lax.broadcasted_iota(jnp.int32, (n_tok, n_tok), 0)
         < lax.broadcasted_iota(jnp.int32, (n_tok, n_tok), 1),
@@ -177,8 +168,8 @@
         return remote(
             outgoing.at[p],
             rows.at[g, y, x, pl.ds(s * chunk, chunk)],
-            disp_send.at[p],
-            disp_recv.at[slot],
+            disp_send,
+            disp_recv.at[g],
             (owner(p), tp),
         )
 
@@ -203,31 +194,30 @@
 
     half = SIDE // 2
     steps = (1, SIDE - 1, 2)
-    ways = (1, SIDE - 1) if FORWARD else steps
-    n_ways = len(ways)
+    ways = (1, SIDE - 1)
 
     def along_light(g, k):
         h, l = place(g)
         ref = one(rows, g, h, l)
-        return remote(ref, ref, a_send.at[g, k], a_recv.at[g, k], peer(g, h, l + steps[k]))
+        return remote(ref, ref, a_send, a_recv.at[g], peer(g, h, l + steps[k]))
 
     def along_heavy(g, k):
         h, l = place(g)
         ref = line(rows, g, h)
-        return remote(ref, ref, b_send.at[g, k], b_recv.at[g, k], peer(g, h + ways[k], l))
+        return remote(ref, ref, b_send, b_recv.at[g, k], peer(g, h + ways[k], l))
 
     def pass_on(g, k):
         h, l = place(g)
         ref = line(rows, g, h + SIDE - ways[k], k * half, half)
-        return remote(ref, ref, c_send.at[g, k], c_recv.at[g, k], peer(g, h + ways[k], l))
+        return remote(ref, ref, c_send, c_recv.at[g], peer(g, h + ways[k], l))
 
     def far_part(g, k):
         h, l = place(g)
         return remote(
             line(part, g, h + 2, k * half, half),
             far_in.at[g, k],
-            far_send.at[g, k],
-            far_recv.at[g, k],
+            far_send,
+            far_recv.at[g],
             peer(g, h + ways[k], l),
         )
 
@@ -236,18 +226,8 @@
         return remote(
             line(part, g, h + ways[k], which * half, half),
             near_in.at[g, k, pl.ds(which * half, half)],
-            near_send.at[g, k, which],
-            near_recv.at[g, k, which],
-            peer(g, h + ways[k], l),
-        )
-
-    def whole_part(g, k):
-        h, l = place(g)
-        return remote(
-            line(part, g, h + ways[k]),
-            near_in.at[g, k],
-            near_send.at[g, k, 0],
-            near_recv.at[g, k, 0],
+            near_send,
+            near_recv.at[g],
             peer(g, h + ways[k], l),
         )
 
@@ -256,48 +236,31 @@
         return remote(
             one(part, g, h, l + steps[k]),
             light_in.at[g, k],
-            light_send.at[g, k],
-            light_recv.at[g, k],
+            light_send,
+            light_recv.at[g],
             peer(g, h, l + steps[k]),
         )
 
     def give_back(p, slot):
         return remote(
-            ret_out.at[p], ret_in.at[slot], ret_send.at[p], ret_recv.at[slot], (owner(p), tp)
-        )
-
-    hops = (1, 2, 4)
-
-    def stage_open(k):
-        if k == 0:
-            pl.semaphore_wait(barrier, len(near) + 2 * (SIDE - 1))
-        else:
-            pl.semaphore_wait(open_sem.at[k - 1], 2)
-        if k < len(hops):
-            for d in (hops[k], n_z - hops[k]):
-                pl.semaphore_signal(
-                    open_sem.at[k],
-                    inc=1,
-                    device_id=(lax.rem(z + d, n_z) * CORES + core, tp),
-                    device_id_type=MESH,
-                )
-        least = hops[k - 1] + 1 if k else 0
-        most = 2 * least - 2 if k else 1
-        for p in range(1, n_ep):
-            if least <= reach(p) <= most:
-                dispatch(p, mirror(p)).start()
+            ret_out.at[p], ret_in.at[slot], ret_send, ret_recv, (owner(p), tp)
+        )
+
+    def arrived(ref, recv):
+        remote(ref, ref, disp_send, recv, (ep, tp)).wait_recv()
+
+    def left(ref, send):
+        remote(ref, ref, send, ret_recv, (ep, tp)).wait_send()
 
     def stage_take(g):
-        for p in range(g * PER, (g + 1) * PER):
-            if p:
-                dispatch(p, p).wait_recv()
+        own = 0 if g else chunk
+        arrived(rows.at[g, y, x, pl.ds(own, block - own)], disp_recv.at[g])
         for k in range(3):
             along_light(g, k).start()
 
     def stage_spread(g):
-        for k in range(3):
-            along_light(g, k).wait_recv()
-        for k in range(n_ways):
+        arrived(rows.at[g, 0, pl.ds(0, len(steps))], a_recv.at[g])
+        for k in range(2):
             along_heavy(g, k).start()
 
     def stage_pass(g):
@@ -306,12 +269,7 @@
             pass_on(g, k).start()
 
     def stage_compute(g):
-        if FORWARD:
-            for k in range(2):
-                pass_on(g, k).wait_recv()
-        else:
-            for k in range(n_ways):
-                along_heavy(g, k).wait_recv()
+        arrived(rows.at[g, 0], c_recv.at[g])
         if g == 0:
             small[3].wait()
         ssq = jnp.zeros((block, cols), jnp.float32)
@@ -346,18 +304,14 @@
                 part[g, q // SIDE, q % SIDE, e * PER * CAP : (e + 1) * PER * CAP] = down[
                     :, q * cols : (q + 1) * cols
                 ]
-        if FORWARD:
-            for k in range(2):
-                far_part(g, k).start()
-                near_part(g, k, 1 - k).start()
-        else:
-            for k in range(n_ways):
-                whole_part(g, k).start()
+        for k in range(2):
+            far_part(g, k).start()
+            near_part(g, k, 1 - k).start()
 
     def stage_join(g):
         h, l = place(g)
+        arrived(far_in.at[g], far_recv.at[g])
         for k in range(2):
-            far_part(g, k).wait_recv()
             mine = line(part, g, h + ways[k], k * half, half)
             mine[...] = (
                 mine[...].astype(jnp.float32) + far_in[g, k].astype(jnp.float32)
@@ -368,12 +322,8 @@
         h, l = place(g)
         mine = line(part, g, h)
         total = mine[...].astype(jnp.float32)
-        for k in range(n_ways):
-            if FORWARD:
-                for which in range(2):
-                    near_part(g, k, which).wait_recv()
-            else:
-                whole_part(g, k).wait_recv()
+        arrived(near_in.at[g], near_recv.at[g])
+        for k in range(2):
             total = total + near_in[g, k].astype(jnp.float32)
         mine[...] = total.astype(jnp.bfloat16)
         for k in range(3):
@@ -382,8 +332,8 @@
     def stage_return(g):
         h, l = place(g)
         total = one(part, g, h, l)[...].astype(jnp.float32)
+        arrived(light_in.at[g], light_recv.at[g])
         for k in range(3):
-            light_part(g, k).wait_recv()
             total = total + light_in[g, k].astype(jnp.float32)
         total = total.reshape(n_exp, PER, CAP, cols)
         back = jnp.stack([total[e] for e in range(n_exp)], axis=1).reshape(PER, chunk, cols)
@@ -403,41 +353,40 @@
         stage_join,
         stage_sum,
         stage_return,
-        stage_open,
     )
+    pl.semaphore_wait(barrier, n_ep - 1 + 2 * (SIDE - 1))
+    for p in range(1, n_ep):
+        dispatch(p, mirror(p)).start()
     for step, (stage, g) in enumerate(PLAN):
         stages[stage](g)
         if step == COMBINE_AT:
+            small[1].wait()
+            weight = jnp.zeros((slots, n_tok), jnp.float32)
+            for k in range(top):
+                hit = rout_ref[k : k + 1, :] == slot_exp
+                weight = weight + jnp.where(hit, gw_ref[k : k + 1, :], 0.0)
             combine[...] = (placing * weight).T
 
     both = combine[...]
     high = both.astype(jnp.bfloat16)
     low = (both - high.astype(jnp.float32)).astype(jnp.bfloat16)
 
-    for p in range(1, n_ep):
-        dispatch(p, mirror(p)).wait_send()
-    for g in range(groups):
-        for k in range(3):
-            along_light(g, k).wait_send()
-            light_part(g, k).wait_send()
-        for k in range(n_ways):
-            along_heavy(g, k).wait_send()
-            if FORWARD:
-                pass_on(g, k).wait_send()
-                far_part(g, k).wait_send()
-                for which in range(2):
-                    near_part(g, k, which).wait_send()
-            else:
-                whole_part(g, k).wait_send()
-    for p in range(1, n_ep):
-        give_back(p, p).wait_recv()
+    others = pl.ds(1, n_ep - 1)
+    left(outgoing.at[others], disp_send)
+    most = groups * len(steps) // SIDE
+    left(rows.at[pl.ds(0, most), 0], a_send)
+    left(rows.at[:, pl.ds(0, 2)], b_send)
+    left(rows.at[:, 0], c_send)
+    left(far_in, far_send)
+    left(near_in, near_send)
+    left(light_in, light_send)
+    arrived(ret_in.at[others], ret_recv)
     back = ret_in[...].reshape(slots, cols)
     out_ref[...] = (
         jnp.dot(high, back, preferred_element_type=jnp.float32)
         + jnp.dot(low, back, preferred_element_type=jnp.float32)
     ).astype(jnp.bfloat16)
-    for p in range(1, n_ep):
-        give_back(p, mirror(p)).wait_send()
+    left(ret_out.at[others], ret_send)
 
 
 def per_device(tokens, routing, gate_weights, norm_gain, w_gate, w_up, w_down):
@@ -468,29 +417,28 @@
             pltpu.VMEM((n_tok, slots), f32),
             pltpu.VMEM((groups, SIDE, SIDE, block, cols), bf16),
             pltpu.VMEM((groups, 2, SIDE // 2, block, cols), bf16),
-            pltpu.VMEM((groups, 3, SIDE, block, cols), bf16),
+            pltpu.VMEM((groups, 2, SIDE, block, cols), bf16),
             pltpu.VMEM((groups, 3, block, cols), bf16),
             pltpu.VMEM((n_ep, chunk, cols), bf16),
             pltpu.VMEM((n_ep, chunk, cols), bf16),
             dma((4,)),
             dma((3, n_exp)),
-            dma((n_ep,)),
-            dma((n_ep,)),
-            dma((groups, 3)),
-            dma((groups, 3)),
-            dma((groups, 3)),
-            dma((groups, 3)),
+            dma,
+            dma((groups,)),
+            dma,
+            dma((groups,)),
+            dma,
             dma((groups, 2)),
-            dma((groups, 2)),
-            dma((groups, 2)),
-            dma((groups, 2)),
-            dma((groups, 3, 2)),
-            dma((groups, 3, 2)),
-            dma((groups, 3)),
-            dma((groups, 3)),
-            dma((n_ep,)),
-            dma((n_ep,)),
-            pltpu.SemaphoreType.REGULAR((3,)),
+            dma,
+            dma((groups,)),
+            dma,
+            dma((groups,)),
+            dma,
+            dma((groups,)),
+            dma,
+            dma((groups,)),
+            dma,
+            dma,
         ],
         compiler_params=pltpu.CompilerParams(collective_id=0, has_side_effects=True),
     )(tokens, routing.T, gate_weights.T, norm_gain.reshape(1, width), w_gate, w_up, w_down)

time: 68.4 us -> 65.3 us (0.955)
  Pallas kernels: 66.9 us -> 63.8 us
    pallas_call x1, Pallas kernels: 66.9 us -> 63.8 us  [per_device(): pl.pallas_call(functools.partial(kernel, n_ep, n_tp), out_shape=jax.Shape...]
where the time goes in v2:
time: 65.3 us; the launch traced here: 65.1 us
  Pallas kernels  63.8 us (98%)
  local copies, waits for them, and re-layouts  1.3 us (2%)
    pallas_call x1, Pallas kernels, per_device(): pl.pallas_call(functools.partial(kernel, n_ep, n_tp), out_shape=jax.Shape...  63.8 us

profile of v2, /device:TPU:1, one launch (start us, length us, event | category | flops | bytes accessed | tf_op | source)
XLA Modules:
  0.0 65.1 jit_solution(18038407002087783365)
XLA Ops:
  0.0 63.8 %shard_map.73 = bf16[32,128]{1,0:T(8,128)(2,1)} custom-call(bf16[32,128]{1,0:T(8,128)(2,1)} %tok_hbm.1, s32[4,32]{1,0:T(4,128)} %bitcast.4, f32[4,32]{1,0:T(4,128)} %bitcast.5, f32[1,2048]{1,0:T(1,128)} %bitcast.3, bf16[2,2048,128]{2,1,0:T(8,128)(2,1)} %wg_hbm.1, bf16[2,2048,128]{2,1,0:T(8,128)(2,1)} %wu_hbm.1, bf16[2,128,2048]{2,1,0:T(8,128)(2,1)} %wd_hbm.1), custom_call_target="tpu_custom_call" | custom-call | tf_op jit(solution)/shard_map/pallas_call | solution.py:403
  63.8 1.3 %copy.9 = bf16[32,128]{1,0:T(8,128)(2,1)} copy(bf16[32,128]{1,0:T(8,128)(2,1)} %shard_map.73) | data formatting | bytes 16384

commit v3 on v2

--- a/solution.py
+++ b/solution.py
@@ -12,7 +12,7 @@
 CORES = 2
 PER = 4
 DZS = (0, 1, -1, 2, -2, 3, -3, 4, 8, 7, -7, 6, -6, 5, -5, -4)
-PLAN = ((0, 0), (0, 1), (0, 2), (0, 3), (1, 0), (0, 7), (0, 6), (0, 5), (1, 1), (0, 4), (1, 2), (1, 3), (2, 0), (1, 6), (2, 1), (1, 7), (1, 5), (1, 4), (2, 2), (2, 3), (3, 0), (3, 1), (2, 6), (2, 7), (2, 4), (2, 5), (3, 2), (3, 3), (4, 0), (4, 1), (3, 6), (3, 7), (3, 4), (3, 5), (4, 2), (4, 3), (5, 0), (5, 1), (4, 6), (4, 7), (4, 4), (4, 5), (5, 2), (5, 3), (6, 1), (5, 6), (6, 0), (5, 7), (5, 4), (5, 5), (6, 2), (6, 3), (6, 6), (6, 7), (6, 4), (6, 5))
+PLAN = ((0, 0), (0, 1), (0, 2), (0, 3), (1, 0), (1, 1), (0, 4), (0, 5), (0, 6), (0, 7), (1, 2), (1, 3), (2, 0), (2, 1), (1, 4), (1, 5), (2, 2), (1, 6), (1, 7), (3, 0), (2, 3), (3, 1), (2, 4), (2, 5), (3, 2), (2, 6), (2, 7), (3, 3), (4, 0), (4, 1), (3, 4), (3, 5), (4, 2), (4, 3), (3, 6), (3, 7), (5, 0), (5, 1), (4, 4), (4, 5), (5, 2), (5, 3), (4, 6), (4, 7), (5, 4), (6, 0), (6, 1), (5, 5), (5, 6), (6, 2), (6, 3), (5, 7), (6, 4), (6, 5), (6, 6), (6, 7))
 COMBINE_AT = 6
 MESH = pl.DeviceIdType.MESH
 
@@ -370,6 +370,7 @@
     both = combine[...]
     high = both.astype(jnp.bfloat16)
     low = (both - high.astype(jnp.float32)).astype(jnp.bfloat16)
+    both = jnp.concatenate([high, low], axis=0)
 
     others = pl.ds(1, n_ep - 1)
     left(outgoing.at[others], disp_send)
@@ -382,10 +383,8 @@
     left(light_in, light_send)
     arrived(ret_in.at[others], ret_recv)
     back = ret_in[...].reshape(slots, cols)
-    out_ref[...] = (
-        jnp.dot(high, back, preferred_element_type=jnp.float32)
-        + jnp.dot(low, back, preferred_element_type=jnp.float32)
-    ).astype(jnp.bfloat16)
+    mixed = jnp.dot(both, back, preferred_element_type=jnp.float32)
+    out_ref[...] = (mixed[:n_tok] + mixed[n_tok:]).astype(jnp.bfloat16)
     left(ret_out.at[others], ret_send)
 
 

time: 65.3 us -> 65.3 us (level)
  no operation moved by 1% of the time
where the time goes in v3:
time: 65.3 us; the launch traced here: 65.1 us
  Pallas kernels  63.8 us (98%)
  local copies, waits for them, and re-layouts  1.3 us (2%)
    pallas_call x1, Pallas kernels, per_device(): pl.pallas_call(functools.partial(kernel, n_ep, n_tp), out_shape=jax.Shape...  63.8 us

profile of v3, /device:TPU:1, one launch (start us, length us, event | category | flops | bytes accessed | tf_op | source)
XLA Modules:
  0.0 65.1 jit_solution(13041284750633773613)
XLA Ops:
  0.0 63.8 %shard_map.73 = bf16[32,128]{1,0:T(8,128)(2,1)} custom-call(bf16[32,128]{1,0:T(8,128)(2,1)} %tok_hbm.1, s32[4,32]{1,0:T(4,128)} %bitcast.4, f32[4,32]{1,0:T(4,128)} %bitcast.5, f32[1,2048]{1,0:T(1,128)} %bitcast.3, bf16[2,2048,128]{2,1,0:T(8,128)(2,1)} %wg_hbm.1, bf16[2,2048,128]{2,1,0:T(8,128)(2,1)} %wu_hbm.1, bf16[2,128,2048]{2,1,0:T(8,128)(2,1)} %wd_hbm.1), custom_call_target="tpu_custom_call" | custom-call | tf_op jit(solution)/shard_map/pallas_call | solution.py:402
  63.8 1.3 %copy.9 = bf16[32,128]{1,0:T(8,128)(2,1)} copy(bf16[32,128]{1,0:T(8,128)(2,1)} %shard_map.73) | data formatting | bytes 16384
